TPU v7x, 32 devices: a whole 2x2x4 slice. The times are simulated.
32 devices in a mesh: fs: 4 (over y, x), tp: 8 (over z, core).
Axes of the slice: x: 2, y: 2, z: 4, core: 2. Of those that a mesh axis runs over, the one named last changes fastest.
Arguments:
- tokens: bfloat16 [2048, 2048], P('fs', 'tp'), may hold values from -6 to 6
- norm_gain: float32 [2048], P('fs'), may hold values from 0.1 to 1.9
- gate_train: float32 [2048, 8192], P('fs', 'tp'), may hold values from -0.125 to 0.125
- up_train: float32 [2048, 8192], P('fs', 'tp'), may hold values from -0.125 to 0.125
- down_train: float32 [8192, 2048], P('fs', 'tp'), may hold values from -0.0625 to 0.0625
Outputs:
- gate_serve: bfloat16 [2048, 8192], P(None, 'tp')
- up_serve: bfloat16 [2048, 8192], P(None, 'tp')
- down_serve: bfloat16 [8192, 2048], P('tp')
- layer_out: bfloat16 [2048, 2048], P(('fs', 'tp'))
All inputs are finite; a program needn't handle non-finite values.
Results may differ from a plain program's by a relative error of at most 0.024.
Values may be sent and summed in bfloat16 or wider, within the bound.
A program may use at most 64 MiB of HBM per device.

v0:
```python
import jax
import jax.numpy as jnp
from jax import lax
from jax.sharding import PartitionSpec as P

D = 2048
epsilon = 1e-06


def body(tokens, norm_gain, gate_train, up_train, down_train):
    gate_local = (norm_gain[:, None] * gate_train).astype(jnp.bfloat16)
    up_local = (norm_gain[:, None] * up_train).astype(jnp.bfloat16)
    down_local = down_train.astype(jnp.bfloat16)
    features = lax.all_gather(tokens, "tp", axis=1, tiled=True)
    wide = features.astype(jnp.float32)
    squares = jnp.sum(wide * wide, axis=1)
    gate_whole, up_whole = (
        lax.all_gather(gate_local, "fs", axis=0, tiled=True),
        lax.all_gather(up_local, "fs", axis=0, tiled=True),
    )
    gate_sum = jnp.dot(features, gate_whole, preferred_element_type=jnp.float32)
    up_sum = jnp.dot(features, up_whole, preferred_element_type=jnp.float32)
    down_rows = lax.all_gather(down_local, "fs", axis=0, tiled=True)
    down_whole = lax.all_to_all(down_rows, "tp", split_axis=0, concat_axis=1, tiled=True)
    scale = lax.rsqrt(squares / D + epsilon)[:, None]
    hidden = (jax.nn.silu(gate_sum * scale) * (up_sum * scale)).astype(jnp.bfloat16)
    mixed = lax.psum_scatter(
        jnp.dot(hidden, down_whole, preferred_element_type=jnp.float32).astype(jnp.bfloat16),
        "tp",
        scatter_dimension=0,
        tiled=True,
    )
    return (gate_whole, up_whole, down_whole, mixed)


def solution(mesh):
    return jax.shard_map(
        body,
        mesh=mesh,
        in_specs=(P("fs", "tp"), P("fs"), P("fs", "tp"), P("fs", "tp"), P("fs", "tp")),
        out_specs=(P(None, "tp"), P(None, "tp"), P("tp", None), P(("fs", "tp"), None)),
        check_vma=False,
    )
```

profile of v0, /device:TPU:0, one launch (start us, length us, event | category | flops | bytes accessed | tf_op | source)
XLA Modules:
  0.0 293.7 jit_solution(2137613969868247611)
XLA Ops:
  7.2 0.0 copy-start.2
  7.2 0.0 copy-start.3
  7.2 0.0 all-gather.9.cloned.1.call-start
  7.2 2.8 convert_element_type.20
  10.0 0.0 all-gather.9.cloned.1.call-update
  10.1 0.0 all-gather.11.cloned.1.call-start
  10.1 0.7 all-gather.11.cloned.1.call-update
  10.8 0.0 all-gather.5.cloned.1.call-start
  10.9 0.0 copy-done.2
  10.9 0.0 copy-done.3
  10.9 3.2 %multiply_convert_fusion = (bf16[512,1024]{1,0:T(8,128)(2,1)}, bf16[512,1024]{1,0:T(8,128)(2,1)}) fusion(f32[512,1024]{1,0:T(8,128)S(1)} %copy-done.2, f32[512]{0:T(512)S(1)} %copy-done.3, f32[512,1024]{1,0:T(8,128)} %param.7), kind=kLoop, calls=%fused_computation.9 | loop fusion | flops 2097152 | bytes 6293504 | tf_op jit(solution)/shard_map/convert_element_type | solution.py:12
  14.1 0.0 all-gather.5.cloned.1.call-update
  14.1 51.6 %all-gather.9.cloned.1.call-done = bf16[8192,256]{1,0:T(8,128)(2,1)} async-done(((bf16[2048,256]{1,0:T(8,128)(2,1)}), bf16[8192,256]{1,0:T(8,128)(2,1)}) %all-gather.9.cloned.1.call-update) | async-done | bytes 4194320 | tf_op jit(solution)/shard_map/all_gather | solution.py:23
  65.7 4.6 %all-to-all-start = ((bf16[8,1024,256]{2,1,0:T(8,128)(2,1)}), bf16[8,1024,256]{2,1,0:T(8,128)(2,1)}, u32[]{:S(2)}, u32[]{:S(2)}) async-start(bf16[8,1024,256]{2,1,0:T(8,128)(2,1)} %bitcast.32), calls=%async_computation | async-start | bytes 8388608 | tf_op jit(solution)/shard_map/all_to_all | solution.py:24
  70.3 0.0 all-gather.7.cloned.1.call-start
  70.4 0.5 all-gather.7.cloned.1.call-update
  70.9 0.0 reduce-scatter.2.cloned.1.call-start
  71.0 50.9 %all-gather.11.cloned.1.call-done = bf16[512,2048]{1,0:T(8,128)(2,1)} async-done(((bf16[512,256]{1,0:T(8,128)(2,1)}), bf16[512,2048]{1,0:T(8,128)(2,1)}) %all-gather.11.cloned.1.call-update) | async-done | bytes 2097168 | tf_op jit(solution)/shard_map/all_gather | solution.py:14
  121.8 2.2 multiply_reduce_fusion
  124.1 54.8 %all-gather.5.cloned.1.call-done = bf16[2048,1024]{1,0:T(8,128)(2,1)} async-done(((bf16[512,1024]{1,0:T(8,128)(2,1)}), bf16[2048,1024]{1,0:T(8,128)(2,1)}) %all-gather.5.cloned.1.call-update) | async-done | bytes 4194320 | tf_op jit(solution)/shard_map/all_gather | solution.py:18
  178.9 0.0 copy-done.1
  178.9 5.9 %fusion.5 = f32[1024,512]{1,0:T(8,128)} fusion(bf16[2048,1024]{1,0:T(8,128)(2,1)} %all-gather.5.cloned.1.call-done, bf16[512,2048]{1,0:T(8,128)(2,1)S(1)} %copy-done.1), kind=kOutput, calls=%fused_computation.13 | convolution fusion | flops 2147483648 | bytes 8388608 | tf_op jit(solution)/shard_map/dot_general | solution.py:21
  184.8 0.0 all-to-all-done
  184.8 6.5 %copy.10 = bf16[8,1024,256]{1,2,0:T(8,128)(2,1)} copy(bf16[8,1024,256]{2,1,0:T(8,128)(2,1)} %all-to-all-done) | data formatting | bytes 8388608 | tf_op jit(solution)/shard_map/all_to_all | solution.py:24
  191.2 42.5 %all-gather.7.cloned.1.call-done = bf16[2048,1024]{1,0:T(8,128)(2,1)} async-done(((bf16[512,1024]{1,0:T(8,128)(2,1)}), bf16[2048,1024]{1,0:T(8,128)(2,1)}) %all-gather.7.cloned.1.call-update) | async-done | bytes 4194320 | tf_op jit(solution)/shard_map/all_gather | solution.py:19
  233.7 10.3 %convolution_convert_fusion = bf16[512,2048]{1,0:T(8,128)(2,1)} fusion(bf16[1024,2048]{0,1:T(8,128)(2,1)} %bitcast.30, f32[1024,512]{1,0:T(8,128)} %fusion.5, bf16[2048,1024]{1,0:T(8,128)(2,1)} %all-gather.7.cloned.1.call-done, bf16[512,2048]{1,0:T(8,128)(2,1)S(1)} %copy-done.1, f32[512]{0:T(512)S(1)} %add_rsqrt_fusion), kind=kOutput, calls=%fused_computation.1 | convolution fusion | flops 4300210176 | bytes 14682112 | tf_op jit(solution)/shard_map/dot_general | solution.py:28
  244.0 0.0 reduce-scatter.2.cloned.1.call-update
  244.0 6.4 %copy.11 = bf16[1024,2048]{1,0:T(8,128)(2,1)} copy(bf16[1024,2048]{0,1:T(8,128)(2,1)} %bitcast.31) | data formatting | bytes 8388608
  250.5 29.8 %reduce-scatter.2.cloned.1.call-done = bf16[64,2048]{1,0:T(8,128)(2,1)} async-done(((bf16[512,2048]{1,0:T(8,128)(2,1)}), bf16[64,2048]{1,0:T(8,128)(2,1)}) %reduce-scatter.2.cloned.1.call-update) | async-done | bytes 262160 | tf_op jit(solution)/shard_map/reduce_scatter | solution.py:27
  280.3 4.8 %copy.14 = bf16[2048,1024]{1,0:T(8,128)(2,1)} copy(bf16[2048,1024]{1,0:T(8,128)(2,1)} %all-gather.5.cloned.1.call-done) | data formatting | bytes 8388608
  285.1 0.0 copy-done
  285.1 2.0 copy.15
  (3 shorter events, 0.0 us)
Async XLA Ops:
  7.2 3.7 %copy-start.2 = (f32[512,1024]{1,0:T(8,128)S(1)}, f32[512,1024]{1,0:T(8,128)}, u32[]{:S(2)}) copy-start(f32[512,1024]{1,0:T(8,128)} %param.8) | copy-start | bytes 6291460
  7.2 3.7 %copy-start.3 = (f32[512]{0:T(512)S(1)}, f32[512]{0:T(512)}, u32[]{:S(2)}) copy-start(f32[512]{0:T(512)} %param.6) | copy-start | bytes 6148
  7.2 58.6 %all-gather.9.cloned.1.call-start = ((), (), s32[]{:S(2)}) async-start(), calls=%async_computation.4 | async-start | bytes 5242880 | tf_op jit(solution)/shard_map/all_gather | solution.py:23
  10.1 111.8 %all-gather.11.cloned.1.call-start = ((), (), s32[]{:S(2)}) async-start(), calls=%async_computation.5 | async-start | bytes 2359296 | tf_op jit(solution)/shard_map/all_gather | solution.py:14
  10.8 168.1 %all-gather.5.cloned.1.call-start = ((), (), s32[]{:S(2)}) async-start(), calls=%async_computation.2 | async-start | bytes 5242880 | tf_op jit(solution)/shard_map/all_gather | solution.py:18
  65.7 119.0 %all-to-all-start = ((bf16[8,1024,256]{2,1,0:T(8,128)(2,1)}), bf16[8,1024,256]{2,1,0:T(8,128)(2,1)}, u32[]{:S(2)}, u32[]{:S(2)}) async-start(bf16[8,1024,256]{2,1,0:T(8,128)(2,1)} %bitcast.32), calls=%async_computation | async-start | bytes 8388608 | tf_op jit(solution)/shard_map/all_to_all | solution.py:24
  70.3 163.4 %all-gather.7.cloned.1.call-start = ((), (), s32[]{:S(2)}) async-start(), calls=%async_computation.3 | async-start | bytes 5242880 | tf_op jit(solution)/shard_map/all_gather | solution.py:19
  70.9 209.4 %reduce-scatter.2.cloned.1.call-start = ((), (), s32[]{:S(2)}) async-start(), calls=%async_computation.6 | async-start | bytes 2359296 | tf_op jit(solution)/shard_map/reduce_scatter | solution.py:27
  121.8 57.0 %copy-start.1 = (bf16[512,2048]{1,0:T(8,128)(2,1)S(1)}, bf16[512,2048]{1,0:T(8,128)(2,1)}, u32[]{:S(2)}) copy-start(bf16[512,2048]{1,0:T(8,128)(2,1)} %all-gather.11.cloned.1.call-done) | copy-start | bytes 6291460
  280.3 4.8 %copy-start = (bf16[2048,1024]{1,0:T(8,128)(2,1)S(1)}, bf16[2048,1024]{1,0:T(8,128)(2,1)}, u32[]{:S(2)}) copy-start(bf16[2048,1024]{1,0:T(8,128)(2,1)} %all-gather.7.cloned.1.call-done) | copy-start | bytes 12582916
Sparse Core Ops, SparseCore 0:
  10.4 55.2 all-gather.8
  67.3 54.4 all-gather.10
  124.3 54.5 all-gather.4
  181.1 52.5 all-gather.6
  244.2 36.0 reduce-scatter.1
where the time goes:
time: 294 us
  waiting for transfers between devices  231 us (79%)
  local copies, waits for them, and re-layouts  19.8 us (7%)
  matrix products  16.2 us (6%)
  between operations  13.8 us (5%)
  other arithmetic  8.23 us (3%)
  starting transfers between devices  4.8 us (2%)
    all_gather x1, waiting for transfers between devices, body(): lax.all_gather(gate_local, 'fs', axis=0, tiled=True)  54.8 us
    all_gather x1, waiting for transfers between devices, body(): down_rows = lax.all_gather(down_local, 'fs', axis=0, tiled=True)  51.6 us
    all_gather x1, waiting for transfers between devices, body(): features = lax.all_gather(tokens, 'tp', axis=1, tiled=True)  50.9 us
    all_gather x1, waiting for transfers between devices, body(): lax.all_gather(up_local, 'fs', axis=0, tiled=True)  42.5 us
    reduce_scatter x1, waiting for transfers between devices, body(): lax.psum_scatter(jnp.dot(hidden, down_whole, preferred_element_type=jnp.f...  29.8 us
    unnamed x11, local copies, waits for them, and re-layouts  13.3 us
    dot_general x1, matrix products, body(): jnp.dot(hidden, down_whole, preferred_element_type=jnp.float32)  10.3 us
    all_to_all x1, local copies, waits for them, and re-layouts, body(): lax.all_to_all(down_rows, 'tp', split_axis=0, concat_axis=1, tiled=True)  6.48 us
  transfers between devices with their start and end apart: 6, of which 5 were waited for; matrix products, arithmetic and copies ran while one was open for 8% of the time, Pallas kernels for 0%

commit v1 on v0

--- a/solution.py
+++ b/solution.py
@@ -11,7 +11,12 @@
     gate_local = (norm_gain[:, None] * gate_train).astype(jnp.bfloat16)
     up_local = (norm_gain[:, None] * up_train).astype(jnp.bfloat16)
     down_local = down_train.astype(jnp.bfloat16)
-    features = lax.all_gather(tokens, "tp", axis=1, tiled=True)
+    ring = [tokens]
+    for hop in range(7):
+        ring.append(lax.ppermute(ring[-1], "tp", [(dev, (dev + 1) % 8) for dev in range(8)]))
+    features = jnp.roll(
+        jnp.concatenate(ring[::-1], axis=1), (lax.axis_index("tp") + 1) * ring[0].shape[1], axis=1
+    )
     wide = features.astype(jnp.float32)
     squares = jnp.sum(wide * wide, axis=1)
     gate_whole, up_whole = (

time: 294 us -> 274 us (0.932)
  waiting for transfers between devices: 231 us -> 193 us
  starting transfers between devices: 4.8 us -> 22.6 us
    ppermute x0 -> x7, waiting for transfers between devices: none -> 106 us  [body(): lax.ppermute(ring[-1], 'tp', [(dev, (dev + 1) % 8) for dev in range(8)])]
    all_gather x1, waiting for transfers between devices: 54.8 us -> 0.02 us  [body(): lax.all_gather(gate_local, 'fs', axis=0, tiled=True)]
    all_gather x1 -> x0, waiting for transfers between devices: 50.9 us -> none  [body(): features = lax.all_gather(tokens, 'tp', axis=1, tiled=True)]
    all_gather x1, waiting for transfers between devices: 42.5 us -> 0.01 us  [body(): lax.all_gather(up_local, 'fs', axis=0, tiled=True)]
    ppermute x0 -> x7, starting transfers between devices: none -> 17.7 us  [body(): lax.ppermute(ring[-1], 'tp', [(dev, (dev + 1) % 8) for dev in range(8)])]
    reduce_scatter x1, waiting for transfers between devices: 29.8 us -> 34.2 us  [body(): lax.psum_scatter(jnp.dot(hidden, down_whole, preferred_element_type=jnp.f...]
    unnamed x11 -> x28, local copies, waits for them, and re-layouts: 13.3 us -> 15.7 us
  transfers between devices with their start and end apart: 6 -> 12, of which waited for: 5 -> 9; matrix products, arithmetic and copies ran while one was open for 8% -> 8% of each run, Pallas kernels for 0% -> 0%
where the time goes in v1:
time: 274 us
  waiting for transfers between devices  193 us (70%)
  starting transfers between devices  22.6 us (8%)
  local copies, waits for them, and re-layouts  22.2 us (8%)
  matrix products  15.3 us (6%)
  between operations  14 us (5%)
  other arithmetic  6.5 us (2%)
    ppermute x7, waiting for transfers between devices, body(): lax.ppermute(ring[-1], 'tp', [(dev, (dev + 1) % 8) for dev in range(8)])  106 us
    all_gather x1, waiting for transfers between devices, body(): down_rows = lax.all_gather(down_local, 'fs', axis=0, tiled=True)  52.4 us
    reduce_scatter x1, waiting for transfers between devices, body(): lax.psum_scatter(jnp.dot(hidden, down_whole, preferred_element_type=jnp.f...  34.2 us
    ppermute x7, starting transfers between devices, body(): lax.ppermute(ring[-1], 'tp', [(dev, (dev + 1) % 8) for dev in range(8)])  17.7 us
    unnamed x28, local copies, waits for them, and re-layouts  15.7 us
    dot_general x1, matrix products, body(): jnp.dot(hidden, down_whole, preferred_element_type=jnp.float32)  10.2 us
    all_to_all x1, local copies, waits for them, and re-layouts, body(): lax.all_to_all(down_rows, 'tp', split_axis=0, concat_axis=1, tiled=True)  6.44 us
  transfers between devices with their start and end apart: 12, of which 9 were waited for; matrix products, arithmetic and copies ran while one was open for 8% of the time, Pallas kernels for 0%

profile of v1, /device:TPU:0, one launch (start us, length us, event | category | flops | bytes accessed | tf_op | source)
XLA Modules:
  0.0 273.6 jit_solution(4316280585949665451)
XLA Ops:
  7.2 0.0 all-gather.8.cloned.1.call-start
  7.2 2.8 %convert_element_type.20 = bf16[2048,256]{1,0:T(8,128)(2,1)} convert(f32[2048,256]{1,0:T(8,128)} %param.9) | non-fusion elementwise | flops 524288 | bytes 3145728 | tf_op jit(solution)/shard_map/convert_element_type | solution.py:13
  10.0 0.0 all-gather.8.cloned.1.call-update
  10.1 0.0 all-gather.4.cloned.1.call-start
  10.1 3.2 %multiply_convert_fusion.1 = (bf16[512,1024]{1,0:T(8,128)(2,1)}, bf16[512,1024]{1,0:T(8,128)(2,1)}) fusion(f32[512,1024]{1,0:T(8,128)S(1)} %copy-done.1, f32[512]{0:T(512)S(1)} %copy-done.4, f32[512,1024]{1,0:T(8,128)} %param.7), kind=kLoop, calls=%fused_computation.3 | loop fusion | flops 2097152 | bytes 6293504 | tf_op jit(solution)/shard_map/convert_element_type | solution.py:12
  13.4 52.4 %all-gather.8.cloned.1.call-done = bf16[8192,256]{1,0:T(8,128)(2,1)} async-done(((bf16[2048,256]{1,0:T(8,128)(2,1)}), bf16[8192,256]{1,0:T(8,128)(2,1)}) %all-gather.8.cloned.1.call-update) | async-done | bytes 4194320 | tf_op jit(solution)/shard_map/all_gather | solution.py:28
  65.7 4.7 %all-to-all-start = ((bf16[8,1024,256]{2,1,0:T(8,128)(2,1)}), bf16[8,1024,256]{2,1,0:T(8,128)(2,1)}, u32[]{:S(2)}, u32[]{:S(2)}) async-start(bf16[8,1024,256]{2,1,0:T(8,128)(2,1)} %bitcast.9), calls=%async_computation | async-start | bytes 8388608 | tf_op jit(solution)/shard_map/all_to_all | solution.py:29
  70.5 0.0 all-gather.6.cloned.1.call-start
  70.5 0.7 all-gather.6.cloned.1.call-update
  71.2 0.0 reduce-scatter.2.cloned.1.call-start
  71.3 0.5 collective-permute-start
  71.8 74.0 %collective-permute-done = bf16[512,256]{1,0:T(8,128)(2,1)S(1)} collective-permute-done((bf16[512,256]{1,0:T(8,128)(2,1)S(1)}, bf16[512,256]{1,0:T(8,128)(2,1)S(1)}, u32[]{:S(2)}, u32[]{:S(2)}) %collective-permute-start) | collective-permute-done | bytes 262176 | tf_op jit(solution)/shard_map/ppermute | solution.py:16
  145.8 7.7 %collective-permute-done.1 = bf16[512,256]{1,0:T(8,128)(2,1)S(1)} collective-permute-done((bf16[512,256]{1,0:T(8,128)(2,1)S(1)}, bf16[512,256]{1,0:T(8,128)(2,1)S(1)}, u32[]{:S(2)}, u32[]{:S(2)}) %collective-permute-start.1) | collective-permute-done | bytes 262176 | tf_op jit(solution)/shard_map/ppermute | solution.py:16
  153.5 7.7 %collective-permute-done.2 = bf16[512,256]{1,0:T(8,128)(2,1)S(1)} collective-permute-done((bf16[512,256]{1,0:T(8,128)(2,1)S(1)}, bf16[512,256]{1,0:T(8,128)(2,1)S(1)}, u32[]{:S(2)}, u32[]{:S(2)}) %collective-permute-start.2) | collective-permute-done | bytes 262176 | tf_op jit(solution)/shard_map/ppermute | solution.py:16
  161.2 9.2 %collective-permute-start.3 = (bf16[512,256]{1,0:T(8,128)(2,1)S(1)}, bf16[512,256]{1,0:T(8,128)(2,1)S(1)}, u32[]{:S(2)}, u32[]{:S(2)}) collective-permute-start(bf16[512,256]{1,0:T(8,128)(2,1)S(1)} %collective-permute-done.2), channel_id=1, source_target_pairs={{0,1},{1,2},{2,3},{3,4},{4,5},{5,6},{6,7},{7,0},{8,9},{9,10},{10,1... | collective-permute-start | bytes 786440 | tf_op jit(solution)/shard_map/ppermute | solution.py:16
  170.5 1.2 collective-permute-done.3
  171.6 4.6 %collective-permute-start.4 = (bf16[512,256]{1,0:T(8,128)(2,1)S(1)}, bf16[512,256]{1,0:T(8,128)(2,1)S(1)}, u32[]{:S(2)}, u32[]{:S(2)}) collective-permute-start(bf16[512,256]{1,0:T(8,128)(2,1)S(1)} %collective-permute-done.3), channel_id=1, source_target_pairs={{0,1},{1,2},{2,3},{3,4},{4,5},{5,6},{6,7},{7,0},{8,9},{9,10},{10,1... | collective-permute-start | bytes 786440 | tf_op jit(solution)/shard_map/ppermute | solution.py:16
  176.3 3.3 %collective-permute-done.4 = bf16[512,256]{1,0:T(8,128)(2,1)S(1)} collective-permute-done((bf16[512,256]{1,0:T(8,128)(2,1)S(1)}, bf16[512,256]{1,0:T(8,128)(2,1)S(1)}, u32[]{:S(2)}, u32[]{:S(2)}) %collective-permute-start.4) | collective-permute-done | bytes 262176 | tf_op jit(solution)/shard_map/ppermute | solution.py:16
  179.5 2.5 collective-permute-start.5
  182.1 5.1 %collective-permute-done.5 = bf16[512,256]{1,0:T(8,128)(2,1)S(1)} collective-permute-done((bf16[512,256]{1,0:T(8,128)(2,1)S(1)}, bf16[512,256]{1,0:T(8,128)(2,1)S(1)}, u32[]{:S(2)}, u32[]{:S(2)}) %collective-permute-start.5) | collective-permute-done | bytes 262176 | tf_op jit(solution)/shard_map/ppermute | solution.py:16
  187.1 0.7 collective-permute-start.6
  187.8 6.9 %collective-permute-done.6 = bf16[512,256]{1,0:T(8,128)(2,1)S(1)} collective-permute-done((bf16[512,256]{1,0:T(8,128)(2,1)S(1)}, bf16[512,256]{1,0:T(8,128)(2,1)S(1)}, u32[]{:S(2)}, u32[]{:S(2)}) %collective-permute-start.6) | collective-permute-done | bytes 262176 | tf_op jit(solution)/shard_map/ppermute | solution.py:16
  195.3 2.0 copy-done.2
  197.3 0.5 multiply_reduce_fusion
  197.8 0.0 all-gather.4.cloned.1.call-done
  197.8 5.2 %fusion.1 = f32[512,1024]{1,0:T(8,128)S(1)} fusion(bf16[2048,1024]{1,0:T(8,128)(2,1)} %all-gather.4.cloned.1.call-done, bf16[512,4096]{1,0:T(8,128)(2,1)} %copy-done.2, s32[]{:T(128)S(6)} %select_n.14), kind=kOutput, calls=%fused_computation.6 | convolution fusion | flops 2147483648 | bytes 8388612 | tf_op jit(solution)/shard_map/dot_general | solution.py:26
  203.0 6.4 %copy.10 = bf16[8,1024,256]{1,2,0:T(8,128)(2,1)} copy(bf16[8,1024,256]{2,1,0:T(8,128)(2,1)} %all-to-all-done) | data formatting | bytes 8388608 | tf_op jit(solution)/shard_map/all_to_all | solution.py:29
  209.4 10.2 %convolution_convert_fusion = bf16[512,2048]{1,0:T(8,128)(2,1)} fusion(bf16[1024,2048]{0,1:T(8,128)(2,1)} %bitcast.7, f32[512,1024]{1,0:T(8,128)S(1)} %fusion.1, bf16[2048,1024]{1,0:T(8,128)(2,1)} %all-gather.6.cloned.1.call-done, bf16[512,4096]{1,0:T(8,128)(2,1)} %copy-done.2, s32[]{:T(128)S(6)} %select_n.14, f32[512]{0:T(512)S(1)} %add_rsqrt_fusion), kind=kOutput, calls=%fused_computation.1 | convolution fusion | flops 4300210176 | bytes 14682116 | tf_op jit(solution)/shard_map/dot_general | solution.py:33
  219.6 6.4 %copy.11 = bf16[1024,2048]{1,0:T(8,128)(2,1)} copy(bf16[1024,2048]{0,1:T(8,128)(2,1)} %bitcast.8) | data formatting | bytes 8388608
  226.1 34.2 %reduce-scatter.2.cloned.1.call-done = bf16[64,2048]{1,0:T(8,128)(2,1)} async-done(((bf16[512,2048]{1,0:T(8,128)(2,1)}), bf16[64,2048]{1,0:T(8,128)(2,1)}) %reduce-scatter.2.cloned.1.call-update) | async-done | bytes 262160 | tf_op jit(solution)/shard_map/reduce_scatter | solution.py:32
  260.2 4.8 %copy.29 = bf16[2048,1024]{1,0:T(8,128)(2,1)} copy(bf16[2048,1024]{1,0:T(8,128)(2,1)} %all-gather.4.cloned.1.call-done) | data formatting | bytes 8388608
  265.0 2.0 copy.30
  (32 shorter events, 0.5 us)
Async XLA Ops:
  7.2 2.9 %copy-start.4 = (f32[512]{0:T(512)S(1)}, f32[512]{0:T(512)}, u32[]{:S(2)}) copy-start(f32[512]{0:T(512)} %param.6) | copy-start | bytes 6148
  7.2 2.9 %copy-start.1 = (f32[512,1024]{1,0:T(8,128)S(1)}, f32[512,1024]{1,0:T(8,128)}, u32[]{:S(2)}) copy-start(f32[512,1024]{1,0:T(8,128)} %param.8) | copy-start | bytes 6291460
  7.2 58.6 %all-gather.8.cloned.1.call-start = ((), (), s32[]{:S(2)}) async-start(), calls=%async_computation.4 | async-start | bytes 5242880 | tf_op jit(solution)/shard_map/all_gather | solution.py:28
  10.1 187.8 %all-gather.4.cloned.1.call-start = ((), (), s32[]{:S(2)}) async-start(), calls=%async_computation.2 | async-start | bytes 5242880 | tf_op jit(solution)/shard_map/all_gather | solution.py:23
  65.7 5.5 %copy-start.3 = (bf16[512,256]{1,0:T(8,128)(2,1)S(1)}, bf16[512,256]{1,0:T(8,128)(2,1)}, u32[]{:S(2)}) copy-start(bf16[512,256]{1,0:T(8,128)(2,1)} %param.5) | copy-start | bytes 786436
  65.7 137.2 %all-to-all-start = ((bf16[8,1024,256]{2,1,0:T(8,128)(2,1)}), bf16[8,1024,256]{2,1,0:T(8,128)(2,1)}, u32[]{:S(2)}, u32[]{:S(2)}) async-start(bf16[8,1024,256]{2,1,0:T(8,128)(2,1)} %bitcast.9), calls=%async_computation | async-start | bytes 8388608 | tf_op jit(solution)/shard_map/all_to_all | solution.py:29
  70.5 139.0 %all-gather.6.cloned.1.call-start = ((), (), s32[]{:S(2)}) async-start(), calls=%async_computation.3 | async-start | bytes 5242880 | tf_op jit(solution)/shard_map/all_gather | solution.py:24
  71.2 189.0 %reduce-scatter.2.cloned.1.call-start = ((), (), s32[]{:S(2)}) async-start(), calls=%async_computation.5 | async-start | bytes 2359296 | tf_op jit(solution)/shard_map/reduce_scatter | solution.py:32
  71.3 74.6 %collective-permute-start = (bf16[512,256]{1,0:T(8,128)(2,1)S(1)}, bf16[512,256]{1,0:T(8,128)(2,1)S(1)}, u32[]{:S(2)}, u32[]{:S(2)}) collective-permute-start(bf16[512,256]{1,0:T(8,128)(2,1)S(1)} %copy-done.3), channel_id=1, source_target_pairs={{0,1},{1,2},{2,3},{3,4},{4,5},{5,6},{6,7},{7,0},{8,9},{9,10},{10,1... | collective-permute-start | bytes 786440 | tf_op jit(solution)/shard_map/ppermute | solution.py:16
  145.8 7.7 %collective-permute-start.1 = (bf16[512,256]{1,0:T(8,128)(2,1)S(1)}, bf16[512,256]{1,0:T(8,128)(2,1)S(1)}, u32[]{:S(2)}, u32[]{:S(2)}) collective-permute-start(bf16[512,256]{1,0:T(8,128)(2,1)S(1)} %collective-permute-done), channel_id=1, source_target_pairs={{0,1},{1,2},{2,3},{3,4},{4,5},{5,6},{6,7},{7,0},{8,9},{9,10},{10,1... | collective-permute-start | bytes 786440 | tf_op jit(solution)/shard_map/ppermute | solution.py:16
  153.5 7.7 %collective-permute-start.2 = (bf16[512,256]{1,0:T(8,128)(2,1)S(1)}, bf16[512,256]{1,0:T(8,128)(2,1)S(1)}, u32[]{:S(2)}, u32[]{:S(2)}) collective-permute-start(bf16[512,256]{1,0:T(8,128)(2,1)S(1)} %collective-permute-done.1), channel_id=1, source_target_pairs={{0,1},{1,2},{2,3},{3,4},{4,5},{5,6},{6,7},{7,0},{8,9},{9,10},{10,1... | collective-permute-start | bytes 786440 | tf_op jit(solution)/shard_map/ppermute | solution.py:16
  161.2 10.4 %collective-permute-start.3 = (bf16[512,256]{1,0:T(8,128)(2,1)S(1)}, bf16[512,256]{1,0:T(8,128)(2,1)S(1)}, u32[]{:S(2)}, u32[]{:S(2)}) collective-permute-start(bf16[512,256]{1,0:T(8,128)(2,1)S(1)} %collective-permute-done.2), channel_id=1, source_target_pairs={{0,1},{1,2},{2,3},{3,4},{4,5},{5,6},{6,7},{7,0},{8,9},{9,10},{10,1... | collective-permute-start | bytes 786440 | tf_op jit(solution)/shard_map/ppermute | solution.py:16
  171.6 7.9 %collective-permute-start.4 = (bf16[512,256]{1,0:T(8,128)(2,1)S(1)}, bf16[512,256]{1,0:T(8,128)(2,1)S(1)}, u32[]{:S(2)}, u32[]{:S(2)}) collective-permute-start(bf16[512,256]{1,0:T(8,128)(2,1)S(1)} %collective-permute-done.3), channel_id=1, source_target_pairs={{0,1},{1,2},{2,3},{3,4},{4,5},{5,6},{6,7},{7,0},{8,9},{9,10},{10,1... | collective-permute-start | bytes 786440 | tf_op jit(solution)/shard_map/ppermute | solution.py:16
  179.5 7.6 %collective-permute-start.5 = (bf16[512,256]{1,0:T(8,128)(2,1)S(1)}, bf16[512,256]{1,0:T(8,128)(2,1)S(1)}, u32[]{:S(2)}, u32[]{:S(2)}) collective-permute-start(bf16[512,256]{1,0:T(8,128)(2,1)S(1)} %collective-permute-done.4), channel_id=1, source_target_pairs={{0,1},{1,2},{2,3},{3,4},{4,5},{5,6},{6,7},{7,0},{8,9},{9,10},{10,1... | collective-permute-start | bytes 786440 | tf_op jit(solution)/shard_map/ppermute | solution.py:16
  187.1 7.6 %collective-permute-start.6 = (bf16[512,256]{1,0:T(8,128)(2,1)S(1)}, bf16[512,256]{1,0:T(8,128)(2,1)S(1)}, u32[]{:S(2)}, u32[]{:S(2)}) collective-permute-start(bf16[512,256]{1,0:T(8,128)(2,1)S(1)} %collective-permute-done.5), channel_id=1, source_target_pairs={{0,1},{1,2},{2,3},{3,4},{4,5},{5,6},{6,7},{7,0},{8,9},{9,10},{10,1... | collective-permute-start | bytes 786440 | tf_op jit(solution)/shard_map/ppermute | solution.py:16
  195.3 2.0 copy-start.2
  260.2 4.8 %copy-start = (bf16[2048,1024]{1,0:T(8,128)(2,1)S(1)}, bf16[2048,1024]{1,0:T(8,128)(2,1)}, u32[]{:S(2)}) copy-start(bf16[2048,1024]{1,0:T(8,128)(2,1)} %all-gather.6.cloned.1.call-done) | copy-start | bytes 12582916
Sparse Core Ops, SparseCore 0:
  10.4 55.2 all-gather.7
  68.2 52.5 all-gather.3
  123.2 52.5 all-gather.5
  219.7 40.4 reduce-scatter.1
